TPU v7x, 256 devices: a 4x2x16 block of a 4x16x16 slice. The times are simulated.
256 devices in a mesh: grp: 2 (over y), fs: 16 (over z), tp: 8 (over x, core).
Axes of the slice: x: 4, y: 2, z: 16, core: 2. Of those that a mesh axis runs over, the one named last changes fastest.
The devices are a block of a 4x16x16 slice.
Arguments:
- incoming_representations: bfloat16 [20480, 2048], P(('grp', 'fs', 'tp')), parts along dimension 0, may hold values from -6 to 6
- perceptron_switch_coefficients: bfloat16 [2048, 5120], P('fs', 'tp'), may hold values from -0.125 to 0.125
- perceptron_expand_coefficients: bfloat16 [2048, 5120], P('fs', 'tp'), may hold values from -0.125 to 0.125
- perceptron_contract_coefficients: bfloat16 [5120, 2048], P('tp', 'fs'), may hold values from -0.5 to 0.5
- probe_coefficients: bfloat16 [2048, 512], P('fs', 'tp'), may hold values from -0.125 to 0.125
- address_coefficients: bfloat16 [2048, 512], P('fs', 'tp'), may hold values from -0.125 to 0.125
- payload_coefficients: bfloat16 [2048, 1024], P('fs', 'tp'), may hold values from -0.125 to 0.125
- emit_switch_coefficients: bfloat16 [2048, 1024], P('fs', 'tp'), may hold values from -0.125 to 0.125
- forgetting_shrink_coefficients: bfloat16 [2048, 32], replicated, may hold values from -0.125 to 0.125
- forgetting_expand_coefficients: bfloat16 [32, 512], P(None, 'tp'), may hold values from -3 to 3
- forgetting_sigmoid_intercept: float32 [512], P('tp'), may hold values from -1 to 9
- extra_forgetting_logits: float32 [20480, 512], P(('grp', 'fs'), 'tp'), parts along dimension 0, may hold values from -0.7 to 0
- subspace_rescaling_amplitude: float32 [128], replicated, may hold values from 0.1 to 1.9
- recurrence_emit_coefficients: bfloat16 [1024, 2048], P('tp', 'fs'), may hold values from -0.5 to 0.5
Outputs:
- layer_out: bfloat16 [20480, 2048], P(('grp', 'fs', 'tp')), parts along dimension 0
There are 2 independent parts, one for each index of `grp`. A program takes and returns all parts, laid end to end along the dimension named above; an argument that names none is the same for every part. Nothing has to cross between parts.
All inputs are finite; a program needn't handle non-finite values.
Results may differ from a plain program's by a relative error of at most 0.035.
Values may be sent and summed in bfloat16 or wider, within the bound.
A program may use at most 64 MiB of HBM per device.

v0:
```python
import jax
import jax.numpy as jnp
from jax import lax
from jax.sharding import PartitionSpec as P

DK = 64
DV = 128
BLOCK = 64
SEQUENCE_LENGTH = 320
residual_gain = 1.681792830507429
forgetting_steepness_multiplier = 16.0
epsilon = 1e-06


def in_order(tiles, dim):
    tiles = jnp.moveaxis(tiles, 0, dim)
    dims = tiles.shape
    return tiles.reshape(*dims[:dim], dims[dim] * dims[dim + 1], *dims[dim + 2 :])


def sent_to_all(x, axis):
    copies = jnp.broadcast_to(x, (lax.axis_size(axis), *x.shape))
    return lax.all_to_all(copies, axis, split_axis=0, concat_axis=0, tiled=True)


def collect(x, axis, dim):
    return in_order(sent_to_all(x, axis), dim)


def cut_along(x, dim, peers):
    dims = x.shape
    tiles = x.reshape(*dims[:dim], peers, dims[dim] // peers, *dims[dim + 1 :])
    return jnp.moveaxis(tiles, dim, 0)


def sent_and_summed(x, axis, dim):
    tiles = cut_along(x, dim, lax.axis_size(axis))
    arrived = lax.all_to_all(tiles, axis, split_axis=0, concat_axis=0, tiled=True)
    return arrived.astype(jnp.float32).sum(axis=0)


def in_one_piece(arrays, axis, dim, along):
    both = jnp.concatenate(arrays, axis=along)
    whole, at, done = (lax.all_gather(both, axis, axis=dim, tiled=True), 0, [])
    for a in arrays:
        done.append(lax.slice_in_dim(whole, at, at + a.shape[along], axis=along))
        at += a.shape[along]
    return tuple(done)


def post_norm(residual, branch):
    summed = residual_gain * residual.astype(jnp.float32) + branch
    average = jnp.mean(summed, axis=-1, keepdims=True)
    centred = summed - average
    variance = jnp.mean(centred * centred, axis=-1, keepdims=True)
    return (centred * lax.rsqrt(variance + epsilon)).astype(jnp.bfloat16)


def gather_group(stored):
    return collect(stored, "tp", 0)


def return_rows(hidden, weight_full):
    return sent_and_summed(
        jnp.dot(hidden, weight_full, preferred_element_type=jnp.float32).astype(jnp.bfloat16),
        "tp",
        0,
    )


def blockwise_mixing(queries, key_rows, values, forgetting_euler_power):
    token_count = queries.shape[0]
    head_count = queries.shape[1] // DK
    seq_count = token_count // SEQUENCE_LENGTH
    block_count = SEQUENCE_LENGTH // BLOCK

    def to_blocks(source, channels):
        shaped = source.astype(jnp.float32).reshape(
            seq_count, block_count, BLOCK, head_count, channels
        )
        return shaped.transpose(0, 3, 1, 2, 4)

    query_blk = to_blocks(queries, DK)
    key_blk = to_blocks(key_rows, DK)
    value_blk = to_blocks(values, DV)
    decay_blk = to_blocks(forgetting_euler_power, DK)
    inclusive = jnp.cumsum(decay_blk, axis=3)
    exclusive = inclusive - decay_blk
    block_end = inclusive[:, :, :, BLOCK - 1 :, :]
    token_positions = jnp.arange(BLOCK)
    lower_mask = (token_positions[:, None] >= token_positions[None, :])[:, :, None]
    flat_lead = seq_count * head_count * block_count

    def flatten(source):
        return source.reshape((flat_lead, BLOCK, source.shape[-1]))

    def within_block(inputs):
        query_one, key_one, value_one, incl_one, excl_one = inputs
        spread = jnp.where(
            lower_mask,
            incl_one[:, None, :] - incl_one[None, :, :],
            excl_one[None, :, :] - excl_one[:, None, :],
        )
        scores = jnp.sum(query_one[:, None, :] * key_one[None, :, :] * jnp.exp(spread), axis=-1)
        return jnp.dot(scores, value_one)

    local_out = lax.map(
        within_block,
        (
            flatten(query_blk),
            flatten(key_blk),
            flatten(value_blk),
            flatten(inclusive),
            flatten(exclusive),
        ),
    )
    local_out = local_out.reshape(value_blk.shape)
    forward_keys = key_blk * jnp.exp(block_end - inclusive)
    backward_keys = key_blk * jnp.exp(exclusive)
    forward_sums = jnp.einsum("shnld,shnlv->nshdv", forward_keys, value_blk)
    backward_sums = jnp.einsum("shnld,shnlv->nshdv", backward_keys, value_blk)
    through = jnp.moveaxis(jnp.exp(block_end[:, :, :, 0, :]), 2, 0)

    def advance(carried, inputs):
        block_sum, segment_passing_across = inputs
        return (segment_passing_across[..., None] * carried + block_sum, carried)

    start_state = jnp.zeros(forward_sums.shape[1:], jnp.float32)
    _, before = lax.scan(advance, start_state, (forward_sums, through))
    _, after = lax.scan(advance, start_state, (backward_sums, through), reverse=True)
    carried_out = jnp.einsum("shnld,nshdv->shnlv", query_blk * jnp.exp(inclusive), before)
    carried_out = carried_out + jnp.einsum(
        "shnld,nshdv->shnlv", query_blk * jnp.exp(block_end - exclusive), after
    )
    combined = local_out + carried_out
    return combined.transpose(0, 2, 3, 1, 4).reshape(token_count, head_count, DV)


def per_device(
    incoming_representations,
    perceptron_switch_coefficients,
    perceptron_expand_coefficients,
    perceptron_contract_coefficients,
    probe_coefficients,
    address_coefficients,
    payload_coefficients,
    emit_switch_coefficients,
    forgetting_shrink_coefficients,
    forgetting_expand_coefficients,
    forgetting_sigmoid_intercept,
    extra_forgetting_logits,
    subspace_rescaling_amplitude,
    recurrence_emit_coefficients,
):
    gate_full, up_full = in_one_piece(
        (perceptron_switch_coefficients, perceptron_expand_coefficients), "fs", 0, 1
    )
    down_kept = lax.all_gather(perceptron_contract_coefficients, "fs", axis=1, tiled=True)

    def expand(gathered):
        return (
            jnp.dot(gathered, gate_full, preferred_element_type=jnp.float32),
            jnp.dot(gathered, up_full, preferred_element_type=jnp.float32),
        )

    def channel_half(stored):
        gathered = gather_group(stored)
        gate_sum, up_sum = expand(gathered)
        hidden = (jax.nn.silu(gate_sum) * up_sum).astype(jnp.bfloat16)
        return post_norm(stored, 0.5 * return_rows(hidden, down_kept))

    opening_perceptron_result = channel_half(incoming_representations)
    gathered = gather_group(opening_perceptron_result)
    pieces = in_one_piece(
        (probe_coefficients, address_coefficients, payload_coefficients, emit_switch_coefficients),
        "fs",
        0,
        1,
    )
    projected = tuple(
        (jnp.dot(gathered, piece_one, preferred_element_type=jnp.float32) for piece_one in pieces)
    )
    queries, key_rows, values, outgate = [summed.astype(jnp.bfloat16) for summed in projected]
    compact_inner_dimensionality = jnp.dot(
        gathered, forgetting_shrink_coefficients, preferred_element_type=jnp.float32
    ).astype(jnp.bfloat16)
    forgetting_euler_power = (
        jax.nn.log_sigmoid(
            jnp.dot(
                compact_inner_dimensionality,
                forgetting_expand_coefficients,
                preferred_element_type=jnp.float32,
            )
            + forgetting_sigmoid_intercept
        )
        / forgetting_steepness_multiplier
        + extra_forgetting_logits
    )
    mixed_heads = blockwise_mixing(queries, key_rows, values, forgetting_euler_power)
    scaled = (
        mixed_heads
        * lax.rsqrt(jnp.mean(mixed_heads * mixed_heads, axis=-1, keepdims=True) + epsilon)
        * subspace_rescaling_amplitude
    )
    opener = jax.nn.silu(outgate.astype(jnp.float32)).reshape(mixed_heads.shape)
    gated = (scaled * opener).reshape(mixed_heads.shape[0], -1).astype(jnp.bfloat16)
    out_full = collect(recurrence_emit_coefficients, "fs", 1)
    context_blend_result = post_norm(opening_perceptron_result, return_rows(gated, out_full))
    return channel_half(context_blend_result)


def solution(mesh):
    return jax.shard_map(
        per_device,
        mesh=mesh,
        in_specs=(
            P(("grp", "fs", "tp"), None),
            P("fs", "tp"),
            P("fs", "tp"),
            P("tp", "fs"),
            P("fs", "tp"),
            P("fs", "tp"),
            P("fs", "tp"),
            P("fs", "tp"),
            P(),
            P(None, "tp"),
            P("tp"),
            P(("grp", "fs"), "tp"),
            P(),
            P("tp", "fs"),
        ),
        out_specs=P(("grp", "fs", "tp"), None),
        check_vma=False,
    )
```

profile of v0, /device:TPU:33, one launch (start us, length us, event | category | flops | bytes accessed | tf_op | source)
XLA Modules:
  0.0 500.8 jit_solution(16295634164969662825)
XLA Ops:
  6.6 1.8 pad_maximum_fusion
  9.2 1.3 broadcast_in_dim.65
  10.5 54.8 %all_to_all.35 = bf16[8,80,2048]{2,1,0:T(8,128)(2,1)S(1)} all-to-all(bf16[8,80,2048]{2,1,0:T(8,128)(2,1)S(1)} %broadcast_in_dim.65), channel_id=1, replica_groups=mesh['grp'=2,'fs'=16,'tp'=8] {'tp'}, dimensions={0} | all-to-all | bytes 5242880 | tf_op jit(solution)/shard_map/all_to_all | solution.py:23
  65.3 29.9 %all-gather.4.cloned.1.call-done = bf16[2048,1280]{1,0:T(8,128)(2,1)} async-done(((bf16[128,1280]{1,0:T(8,128)(2,1)}), bf16[2048,1280]{1,0:T(8,128)(2,1)}) %all-gather.4.cloned.1.call-update) | async-done | bytes 5242896 | tf_op jit(solution)/shard_map/all_gather | solution.py:44
  95.1 5.1 %fusion.15 = f32[640,640]{1,0:T(8,128)} fusion(bf16[640,2048]{1,0:T(8,128)(2,1)S(1)} %bitcast.213, bf16[2048,1280]{1,0:T(8,128)(2,1)} %all-gather.4.cloned.1.call-done), kind=kOutput, calls=%fused_computation.35 | convolution fusion | flops 1677721600 | bytes 6881280 | tf_op jit(solution)/shard_map/dot_general | solution.py:162
  100.3 70.1 %all-gather.6.cloned.1.call-done = bf16[640,2048]{1,0:T(8,128)(2,1)} async-done(((bf16[640,128]{1,0:T(8,128)(2,1)}), bf16[640,2048]{1,0:T(8,128)(2,1)}) %all-gather.6.cloned.1.call-update) | async-done | bytes 2621456 | tf_op jit(solution)/shard_map/all_gather | solution.py:158
  170.3 12.9 %convolution_convert_fusion.1 = bf16[640,2048]{1,0:T(8,128)(2,1)} fusion(bf16[640,2048]{1,0:T(8,128)(2,1)} %all-gather.6.cloned.1.call-done, f32[640,640]{1,0:T(8,128)} %fusion.15, bf16[640,2048]{1,0:T(8,128)(2,1)S(1)} %bitcast.214, bf16[2048,1280]{1,0:T(8,128)(2,1)} %all-gather.4.cloned.1.call-done), kind=kOutput, calls=%fused_computation.27 | convolution fusion | flops 3359211520 | bytes 12124160 | tf_op jit(solution)/shard_map/dot_general | solution.py:65
  183.2 16.1 %all-to-all-start.1 = ((bf16[8,80,2048]{2,1,0:T(8,128)(2,1)}), bf16[8,80,2048]{2,1,0:T(8,128)(2,1)S(1)}, u32[]{:S(2)}, u32[]{:S(2)}) async-start(bf16[8,80,2048]{2,1,0:T(8,128)(2,1)} %bitcast.212), calls=%async_computation.1 | async-start | bytes 5242880 | tf_op jit(solution)/shard_map/all_to_all | solution.py:38
  200.4 30.8 %all-to-all-done.1 = bf16[8,80,2048]{2,1,0:T(8,128)(2,1)S(1)} async-done(((bf16[8,80,2048]{2,1,0:T(8,128)(2,1)}), bf16[8,80,2048]{2,1,0:T(8,128)(2,1)S(1)}, u32[]{:S(2)}, u32[]{:S(2)}) %all-to-all-start.1) | async-done | bytes 2621472 | tf_op jit(solution)/shard_map/all_to_all | solution.py:38
  232.3 1.9 broadcast_in_dim.67
  234.2 4.6 all-to-all-start.2
  239.0 31.8 %all-to-all-done.2 = bf16[8,80,2048]{2,1,0:T(8,128)(2,1)S(1)} async-done(((bf16[8,80,2048]{2,1,0:T(8,128)(2,1)}), bf16[8,80,2048]{2,1,0:T(8,128)(2,1)S(1)}, u32[]{:S(2)}, u32[]{:S(2)}) %all-to-all-start.2) | async-done | bytes 2621472 | tf_op jit(solution)/shard_map/all_to_all | solution.py:23
  270.7 1.0 broadcast_in_dim.69
  271.7 7.1 %all-to-all-start.3 = ((bf16[16,128,128]{1,2,0:T(8,128)(2,1)}), bf16[16,128,128]{1,2,0:T(8,128)(2,1)}, u32[]{:S(2)}, u32[]{:S(2)}) async-start(bf16[16,128,128]{1,2,0:T(8,128)(2,1)} %broadcast_in_dim.69), calls=%async_computation.3 | async-start | bytes 1048576 | tf_op jit(solution)/shard_map/all_to_all | solution.py:23
  278.9 2.0 fusion.29
  280.8 0.9 copy.77
  281.8 2.0 fusion.28
  284.7 1.1 fusion.60
  286.7 1.3 reduce_window_sum.13
  288.6 1.7 bitcast_subtract_fusion.3
  290.3 2.5 convolution_convert_fusion.4
  292.9 44.2 %while.41 = (s32[]{:T(128)}, f32[10,64,128]{2,1,0:T(8,128)}, f32[10,64,64]{2,1,0:T(8,128)}, f32[10,64,64]{2,1,0:T(8,128)}, f32[10,64,64]{2,1,0:T(8,128)S(1)}, /*...) while((s32[]{:T(128)}, f32[10,64,128]{2,1,0:T(8,128)}, ...), condition=%wide.region_6.7_spmd.clone, body=%wide.region_4.6_spmd.clone.sunk | while | flops 2621442 | bytes 271461 | solution.py:107
  294.4 1.4 multiply_reduce_fusion.6
  295.8 1.5 fusion.96
  298.9 1.4 multiply_reduce_fusion.6
  300.3 1.5 fusion.96
  303.3 1.4 multiply_reduce_fusion.6
  304.7 1.5 fusion.96
  307.7 1.4 multiply_reduce_fusion.6
  309.1 1.5 fusion.96
  312.1 1.4 multiply_reduce_fusion.6
  313.5 1.5 fusion.96
  316.5 1.4 multiply_reduce_fusion.6
  317.9 1.5 fusion.96
  321.0 1.4 multiply_reduce_fusion.6
  322.4 1.5 fusion.96
  325.4 1.4 multiply_reduce_fusion.6
  326.8 1.5 fusion.96
  329.8 1.4 multiply_reduce_fusion.6
  331.2 1.5 fusion.96
  334.2 1.4 multiply_reduce_fusion.6
  335.6 1.5 fusion.96
  337.8 1.2 exponential_multiply_fusion
  339.0 1.9 convolution_bitcast_fusion.2
  340.9 1.9 convolution_bitcast_fusion.1
  343.5 7.9 %while.43 = (s32[]{:T(128)}, f32[2,1,64,128]{3,2,1,0:T(8,128)S(1)}, bf16[5,2,1,64,128]{4,3,1,2,0:T(8,128)(2,1)}, f32[5,2,1,64]{3,1,2,0:T(2,128)S(1)}, f32[5,2,1,...) while((s32[]{:T(128)}, f32[2,1,64,128]{3,2,1,0:T(8,128)S(1)}, ...), condition=%wide.region_10.11_spmd.clone, body=%wide.region_9.10_spmd.clone.sunk | while | flops 65540 | bytes 296576 | solution.py:130
  344.1 0.9 fusion.98
  345.7 0.9 fusion.98
  347.3 0.9 fusion.98
  348.8 0.9 fusion.98
  350.4 0.9 fusion.98
  352.1 7.8 %while.42 = (s32[]{:T(128)}, f32[2,1,64,128]{3,2,1,0:T(8,128)S(1)}, bf16[5,2,1,64,128]{4,3,1,2,0:T(8,128)(2,1)}, f32[5,2,1,64]{3,1,2,0:T(2,128)S(1)}, f32[5,2,1,64,128]{4,3,1,2,0:T(8,128)}, /*index=5*/s32[]{:T(128)}, s32[]{:T(128)}) while((s32[]{:T(128)}, f32[2,1,64,128]{3,2,1,0:T(8,128)S(1)}, ...), condition=%wide.region_8.9_spmd.clone, body=%wide.region_7.8_spmd.clone.sunk | while | flops 65539 | bytes 296556 | solution.py:129
  352.7 0.9 fusion.97
  354.2 0.9 fusion.97
  355.8 0.9 fusion.97
  359.9 1.2 fusion.46
  361.1 2.2 multiply_reduce_fusion.4
  363.4 2.0 fusion.42
  365.4 1.9 convolution_convert_fusion.2
  367.3 35.6 %all_to_all.36 = bf16[8,80,2048]{2,1,0:T(8,128)(2,1)S(1)} all-to-all(bf16[8,80,2048]{2,1,0:T(8,128)(2,1)S(1)} %bitcast.200), channel_id=1, replica_groups=mesh['grp'=2,'fs'=16,'tp'=8] {'tp'}, dimensions={0} | all-to-all | bytes 5242880 | tf_op jit(solution)/shard_map/all_to_all | solution.py:38
  404.2 35.5 %all_to_all.37 = bf16[8,80,2048]{2,1,0:T(8,128)(2,1)S(1)} all-to-all(bf16[8,80,2048]{2,1,0:T(8,128)(2,1)S(1)} %broadcast_in_dim.70), channel_id=1, replica_groups=mesh['grp'=2,'fs'=16,'tp'=8] {'tp'}, dimensions={0} | all-to-all | bytes 5242880 | tf_op jit(solution)/shard_map/all_to_all | solution.py:23
  439.8 3.4 fusion.13
  443.1 12.9 %convolution_convert_fusion = bf16[640,2048]{1,0:T(8,128)(2,1)} fusion(bf16[640,2048]{1,0:T(8,128)(2,1)} %all-gather.6.cloned.1.call-done, f32[640,640]{0,1:T(8,128)} %fusion.13, bf16[640,2048]{1,0:T(8,128)(2,1)S(1)} %bitcast.216, bf16[2048,1280]{1,0:T(8,128)(2,1)} %all-gather.4.cloned.1.call-done), kind=kOutput, calls=%fused_computation.26 | convolution fusion | flops 3359211520 | bytes 12124160 | tf_op jit(solution)/shard_map/dot_general | solution.py:65
  456.0 36.4 %all_to_all.38 = bf16[8,80,2048]{2,1,0:T(8,128)(2,1)S(1)} all-to-all(bf16[8,80,2048]{2,1,0:T(8,128)(2,1)} %bitcast.217), channel_id=1, replica_groups=mesh['grp'=2,'fs'=16,'tp'=8] {'tp'}, dimensions={0} | all-to-all | bytes 5242880 | tf_op jit(solution)/shard_map/all_to_all | solution.py:38
  (123 shorter events, 34.5 us)
Async XLA Ops:
  6.5 278.2 %copy-start = (bf16[2048,32]{0,1:T(8,128)(2,1)S(1)}, bf16[2048,32]{0,1:T(8,128)(2,1)}, u32[]{:S(2)}) copy-start(bf16[2048,32]{0,1:T(8,128)(2,1)} %param.28) | copy-start | bytes 393220
  6.6 88.6 %all-gather.4.cloned.1.call-start = ((), (), s32[]{:S(2)}) async-start(), calls=%async_computation.7 | async-start | bytes 5570560 | tf_op jit(solution)/shard_map/all_gather | solution.py:44
  8.4 161.9 %all-gather.6.cloned.1.call-start = ((), (), s32[]{:S(2)}) async-start(), calls=%async_computation.8 | async-start | bytes 2785280 | tf_op jit(solution)/shard_map/all_gather | solution.py:158
  183.2 16.2 %copy-start.6 = (bf16[128,64]{0,1:T(8,128)(2,1)S(1)}, bf16[128,64]{0,1:T(8,128)(2,1)}, u32[]{:S(2)}) copy-start(bf16[128,64]{0,1:T(8,128)(2,1)} %param.25) | copy-start | bytes 49156
  183.2 16.3 %copy-start.7 = (bf16[128,64]{0,1:T(8,128)(2,1)S(1)}, bf16[128,64]{0,1:T(8,128)(2,1)}, u32[]{:S(2)}) copy-start(bf16[128,64]{0,1:T(8,128)(2,1)} %param.24) | copy-start | bytes 49156
  183.2 16.4 %copy-start.3 = (bf16[128,128]{1,0:T(8,128)(2,1)S(1)}, bf16[128,128]{1,0:T(8,128)(2,1)}, u32[]{:S(2)}) copy-start(bf16[128,128]{1,0:T(8,128)(2,1)} %param.27) | copy-start | bytes 98308
  183.2 16.4 %copy-start.4 = (bf16[128,128]{1,0:T(8,128)(2,1)S(1)}, bf16[128,128]{1,0:T(8,128)(2,1)}, u32[]{:S(2)}) copy-start(bf16[128,128]{1,0:T(8,128)(2,1)} %param.26) | copy-start | bytes 98308
  183.2 48.0 %all-to-all-start.1 = ((bf16[8,80,2048]{2,1,0:T(8,128)(2,1)}), bf16[8,80,2048]{2,1,0:T(8,128)(2,1)S(1)}, u32[]{:S(2)}, u32[]{:S(2)}) async-start(bf16[8,80,2048]{2,1,0:T(8,128)(2,1)} %bitcast.212), calls=%async_computation.1 | async-start | bytes 5242880 | tf_op jit(solution)/shard_map/all_to_all | solution.py:38
  199.3 32.3 %copy-start.1 = (bf16[80,2048]{1,0:T(8,128)(2,1)S(1)}, bf16[80,2048]{1,0:T(8,128)(2,1)}, u32[]{:S(2)}) copy-start(bf16[80,2048]{1,0:T(8,128)(2,1)} %param.20) | copy-start | bytes 983044
  199.3 79.5 %all-gather.8.cloned.1.call-start = ((), (), s32[]{:S(2)}) async-start(), calls=%async_computation.9 | async-start | bytes 1671168 | tf_op jit(solution)/shard_map/all_gather | solution.py:44
  234.2 4.7 copy-start.5
  234.2 36.6 %all-to-all-start.2 = ((bf16[8,80,2048]{2,1,0:T(8,128)(2,1)}), bf16[8,80,2048]{2,1,0:T(8,128)(2,1)S(1)}, u32[]{:S(2)}, u32[]{:S(2)}) async-start(bf16[8,80,2048]{2,1,0:T(8,128)(2,1)} %broadcast_in_dim.67), calls=%async_computation.2 | async-start | bytes 5242880 | tf_op jit(solution)/shard_map/all_to_all | solution.py:23
  271.7 93.7 %all-to-all-start.3 = ((bf16[16,128,128]{1,2,0:T(8,128)(2,1)}), bf16[16,128,128]{1,2,0:T(8,128)(2,1)}, u32[]{:S(2)}, u32[]{:S(2)}) async-start(bf16[16,128,128]{1,2,0:T(8,128)(2,1)} %broadcast_in_dim.69), calls=%async_computation.3 | async-start | bytes 1048576 | tf_op jit(solution)/shard_map/all_to_all | solution.py:23
  280.8 3.9 copy-start.2
  280.8 3.9 copy-start.8
  280.8 3.9 copy-start.9
  351.4 12.0 %copy-start.10 = (f32[128]{0:T(128)S(1)}, f32[128]{0:T(128)}, u32[]{:S(2)}) copy-start(f32[128]{0:T(128)} %param.32) | copy-start | bytes 1540
  403.3 36.5 %slice-start = ((s8[5242880]{0:T(1024)(128)(4,1)}), s8[4194304]{0:T(1024)(128)(4,1)S(1)}, s32[]{:S(2)}) async-start(s8[5242880]{0:T(1024)(128)(4,1)} %bitcast.225), calls=%async_computation.10 | async-start | bytes 8388608
  403.9 35.8 %slice-start.1 = ((s8[5242880]{0:T(1024)(128)(4,1)}), s8[1048576]{0:T(1024)(128)(4,1)S(1)}, s32[]{:S(2)}) async-start(s8[5242880]{0:T(1024)(128)(4,1)} %bitcast.225), calls=%async_computation.11 | async-start | bytes 2097152
Sparse Core Ops, SparseCore 0:
  9.1 85.9 all-gather.3
  96.9 73.4 all-gather.5
  201.9 56.6 all-gather.7
where the time goes:
time: 504 us; the launch traced here: 501 us
  waiting for transfers between devices  163 us (32%)
  blocking collectives  162 us (32%)
  matrix products  67.5 us (13%)
  other arithmetic  40.3 us (8%)
  starting transfers between devices  28 us (6%)
  local copies, waits for them, and re-layouts  25.8 us (5%)
  between operations  13.4 us (3%)
    all_to_all x2, blocking collectives, sent_to_all(): return lax.all_to_all(copies, axis, split_axis=0, concat_axis=0, tiled=True)  90.3 us
    all_to_all x2, blocking collectives, sent_and_summed(): lax.all_to_all(tiles, axis, split_axis=0, concat_axis=0, tiled=True)  72 us
    all_gather x1, waiting for transfers between devices, per_device(): lax.all_gather(perceptron_contract_coefficients, 'fs', axis=1, tiled=True)  70.1 us
    all_to_all x2, waiting for transfers between devices, sent_to_all(): return lax.all_to_all(copies, axis, split_axis=0, concat_axis=0, tiled=True)  31.8 us
    all_to_all x1, waiting for transfers between devices, sent_and_summed(): lax.all_to_all(tiles, axis, split_axis=0, concat_axis=0, tiled=True)  30.8 us
    all_gather x2, waiting for transfers between devices, in_one_piece(): whole, at, done = (lax.all_gather(both, axis, axis=dim, tiled=True), 0, [])  29.9 us
    dot_general x3, matrix products, return_rows(): jnp.dot(hidden, weight_full, preferred_element_type=jnp.float32)  27.6 us
    all_to_all x1, starting transfers between devices, sent_and_summed(): lax.all_to_all(tiles, axis, split_axis=0, concat_axis=0, tiled=True)  16.1 us
  transfers between devices with their start and end apart: 6, of which 4 were waited for; matrix products, arithmetic and copies ran while one was open for 19% of the time, Pallas kernels for 0%

commit v1 on v0

--- a/solution.py
+++ b/solution.py
@@ -155,7 +155,15 @@
     gate_full, up_full = in_one_piece(
         (perceptron_switch_coefficients, perceptron_expand_coefficients), "fs", 0, 1
     )
-    down_kept = lax.all_gather(perceptron_contract_coefficients, "fs", axis=1, tiled=True)
+    down_kept = jnp.concatenate(
+        jax.lax.all_to_all(
+            jnp.stack(jax.lax.axis_size("fs") * [perceptron_contract_coefficients]),
+            axis_name="fs",
+            split_axis=0,
+            concat_axis=0,
+        ),
+        1,
+    )
 
     def expand(gathered):
         return (

time: 504 us -> 546 us (1.083)
  waiting for transfers between devices: 163 us -> 235 us
  blocking collectives: 162 us -> 107 us
  starting transfers between devices: 28 us -> 52.3 us
  local copies, waits for them, and re-layouts: 25.8 us -> 31.4 us
    all_gather x2, waiting for transfers between devices: 29.9 us -> 142 us  [in_one_piece(): whole, at, done = (lax.all_gather(both, axis, axis=dim, tiled=True), 0, [])]
    all_gather x1 -> x0, waiting for transfers between devices: 70.1 us -> none  [per_device(): lax.all_gather(perceptron_contract_coefficients, 'fs', axis=1, tiled=True)]
    all_to_all x2 -> x1, blocking collectives: 90.3 us -> 35.5 us  [sent_to_all(): return lax.all_to_all(copies, axis, split_axis=0, concat_axis=0, tiled=True)]
    all_to_all x2 -> x3, waiting for transfers between devices: 31.8 us -> 62.7 us  [sent_to_all(): return lax.all_to_all(copies, axis, split_axis=0, concat_axis=0, tiled=True)]
    all_to_all x2 -> x3, starting transfers between devices: 11.8 us -> 36.5 us  [sent_to_all(): return lax.all_to_all(copies, axis, split_axis=0, concat_axis=0, tiled=True)]
    all_to_all x1, starting transfers between devices: 16.1 us -> 10.1 us  [sent_and_summed(): lax.all_to_all(tiles, axis, split_axis=0, concat_axis=0, tiled=True)]
    all_to_all x0 -> x1, starting transfers between devices: none -> 5.67 us  [per_device(): jax.lax.all_to_all(jnp.stack(jax.lax.axis_size('fs') * [perceptron_contra...]
  transfers between devices with their start and end apart: 6 -> 7, of which waited for: 4 -> 4; matrix products, arithmetic and copies ran while one was open for 19% -> 18% of each run, Pallas kernels for 0% -> 0%
where the time goes in v1:
time: 546 us; the launch traced here: 543 us
  waiting for transfers between devices  235 us (43%)
  blocking collectives  107 us (20%)
  matrix products  63.2 us (12%)
  starting transfers between devices  52.3 us (10%)
  other arithmetic  39.2 us (7%)
  local copies, waits for them, and re-layouts  31.4 us (6%)
  between operations  13.7 us (3%)
    all_gather x2, waiting for transfers between devices, in_one_piece(): whole, at, done = (lax.all_gather(both, axis, axis=dim, tiled=True), 0, [])  142 us
    all_to_all x2, blocking collectives, sent_and_summed(): lax.all_to_all(tiles, axis, split_axis=0, concat_axis=0, tiled=True)  72 us
    all_to_all x3, waiting for transfers between devices, sent_to_all(): return lax.all_to_all(copies, axis, split_axis=0, concat_axis=0, tiled=True)  62.7 us
    all_to_all x3, starting transfers between devices, sent_to_all(): return lax.all_to_all(copies, axis, split_axis=0, concat_axis=0, tiled=True)  36.5 us
    all_to_all x1, blocking collectives, sent_to_all(): return lax.all_to_all(copies, axis, split_axis=0, concat_axis=0, tiled=True)  35.5 us
    all_to_all x1, waiting for transfers between devices, sent_and_summed(): lax.all_to_all(tiles, axis, split_axis=0, concat_axis=0, tiled=True)  30.7 us
    dot_general x3, matrix products, return_rows(): jnp.dot(hidden, weight_full, preferred_element_type=jnp.float32)  22.4 us
    dot_general x10, matrix products, within_block(): return jnp.dot(scores, value_one)  14.6 us
  transfers between devices with their start and end apart: 7, of which 4 were waited for; matrix products, arithmetic and copies ran while one was open for 18% of the time, Pallas kernels for 0%

profile of v1, /device:TPU:33, one launch (start us, length us, event | category | flops | bytes accessed | tf_op | source)
XLA Modules:
  0.0 542.9 jit_solution(3959074983749930419)
XLA Ops:
  6.6 2.8 broadcast_in_dim.65
  9.4 24.1 %all-to-all-start = ((bf16[8,80,2048]{2,1,0:T(8,128)(2,1)}), bf16[8,80,2048]{2,1,0:T(8,128)(2,1)S(1)}, u32[]{:S(2)}, u32[]{:S(2)}) async-start(bf16[8,80,2048]{2,1,0:T(8,128)(2,1)} %broadcast_in_dim.65), calls=%async_computation | async-start | bytes 5242880 | tf_op jit(solution)/shard_map/all_to_all | solution.py:23
  34.5 30.9 %all-to-all-done = bf16[8,80,2048]{2,1,0:T(8,128)(2,1)S(1)} async-done(((bf16[8,80,2048]{2,1,0:T(8,128)(2,1)}), bf16[8,80,2048]{2,1,0:T(8,128)(2,1)S(1)}, u32[]{:S(2)}, u32[]{:S(2)}) %all-to-all-start) | async-done | bytes 2621472 | tf_op jit(solution)/shard_map/all_to_all | solution.py:23
  65.4 2.0 stack.2
  67.7 5.7 %all-to-all-start.1 = ((bf16[16,640,128]{1,2,0:T(8,128)(2,1)}), bf16[16,640,128]{1,2,0:T(8,128)(2,1)S(1)}, u32[]{:S(2)}, u32[]{:S(2)}) async-start(bf16[16,640,128]{1,2,0:T(8,128)(2,1)} %stack.2), calls=%async_computation.1 | async-start | bytes 5242880 | tf_op jit(solution)/shard_map/all_to_all | solution.py:159
  73.4 141.8 %all-gather.3.cloned.1.call-done = bf16[2048,1280]{1,0:T(8,128)(2,1)} async-done(((bf16[128,1280]{1,0:T(8,128)(2,1)}), bf16[2048,1280]{1,0:T(8,128)(2,1)}) %all-gather.3.cloned.1.call-update) | async-done | bytes 5242896 | tf_op jit(solution)/shard_map/all_gather | solution.py:44
  215.2 6.0 %fusion.15 = f32[640,640]{1,0:T(8,128)} fusion(bf16[640,2048]{1,0:T(8,128)(2,1)} %bitcast.217, bf16[2048,1280]{1,0:T(8,128)(2,1)} %all-gather.3.cloned.1.call-done), kind=kOutput, calls=%fused_computation.35 | convolution fusion | flops 1677721600 | bytes 6881280 | tf_op jit(solution)/shard_map/dot_general | solution.py:170
  221.2 10.8 %convolution_convert_fusion.1 = bf16[640,2048]{1,0:T(8,128)(2,1)} fusion(bf16[640,2048]{0,1:T(8,128)(2,1)S(1)} %bitcast.215, f32[640,640]{1,0:T(8,128)} %fusion.15, bf16[640,2048]{1,0:T(8,128)(2,1)} %bitcast.218, bf16[2048,1280]{1,0:T(8,128)(2,1)} %all-gather.3.cloned.1.call-done), kind=kOutput, calls=%fused_computation.27 | convolution fusion | flops 3359211520 | bytes 12124160 | tf_op jit(solution)/shard_map/dot_general | solution.py:65
  232.0 10.1 %all-to-all-start.2 = ((bf16[8,80,2048]{2,1,0:T(8,128)(2,1)}), bf16[8,80,2048]{2,1,0:T(8,128)(2,1)S(1)}, u32[]{:S(2)}, u32[]{:S(2)}) async-start(bf16[8,80,2048]{2,1,0:T(8,128)(2,1)} %bitcast.219), calls=%async_computation.2 | async-start | bytes 5242880 | tf_op jit(solution)/shard_map/all_to_all | solution.py:38
  243.2 30.7 %all-to-all-done.2 = bf16[8,80,2048]{2,1,0:T(8,128)(2,1)S(1)} async-done(((bf16[8,80,2048]{2,1,0:T(8,128)(2,1)}), bf16[8,80,2048]{2,1,0:T(8,128)(2,1)S(1)}, u32[]{:S(2)}, u32[]{:S(2)}) %all-to-all-start.2) | async-done | bytes 2621472 | tf_op jit(solution)/shard_map/all_to_all | solution.py:38
  275.1 1.9 broadcast_in_dim.67
  276.9 4.6 all-to-all-start.3
  281.7 31.8 %all-to-all-done.3 = bf16[8,80,2048]{2,1,0:T(8,128)(2,1)S(1)} async-done(((bf16[8,80,2048]{2,1,0:T(8,128)(2,1)}), bf16[8,80,2048]{2,1,0:T(8,128)(2,1)S(1)}, u32[]{:S(2)}, u32[]{:S(2)}) %all-to-all-start.3) | async-done | bytes 2621472 | tf_op jit(solution)/shard_map/all_to_all | solution.py:23
  313.5 0.9 broadcast_in_dim.69
  314.4 7.8 %all-to-all-start.4 = ((bf16[16,128,128]{1,2,0:T(8,128)(2,1)}), bf16[16,128,128]{1,2,0:T(8,128)(2,1)}, u32[]{:S(2)}, u32[]{:S(2)}) async-start(bf16[16,128,128]{1,2,0:T(8,128)(2,1)} %broadcast_in_dim.69), calls=%async_computation.4 | async-start | bytes 1048576 | tf_op jit(solution)/shard_map/all_to_all | solution.py:23
  322.3 2.0 fusion.29
  324.3 0.9 copy.79
  325.2 2.0 fusion.28
  328.2 1.1 fusion.60
  330.2 1.3 reduce_window_sum.13
  332.0 1.7 bitcast_subtract_fusion.3
  333.8 2.6 convolution_convert_fusion.4
  336.3 44.2 %while.41 = (s32[]{:T(128)}, f32[10,64,128]{2,1,0:T(8,128)}, f32[10,64,64]{2,1,0:T(8,128)}, f32[10,64,64]{2,1,0:T(8,128)}, f32[10,64,64]{2,1,0:T(8,128)S(1)}, /*...) while((s32[]{:T(128)}, f32[10,64,128]{2,1,0:T(8,128)}, ...), condition=%wide.region_6.7_spmd.clone, body=%wide.region_4.6_spmd.clone.sunk | while | flops 2621442 | bytes 271461 | solution.py:107
  337.9 1.4 multiply_reduce_fusion.6
  339.3 1.5 fusion.96
  342.3 1.4 multiply_reduce_fusion.6
  343.7 1.5 fusion.96
  346.7 1.4 multiply_reduce_fusion.6
  348.1 1.5 fusion.96
  351.1 1.4 multiply_reduce_fusion.6
  352.5 1.5 fusion.96
  355.6 1.4 multiply_reduce_fusion.6
  357.0 1.5 fusion.96
  360.0 1.4 multiply_reduce_fusion.6
  361.4 1.5 fusion.96
  364.4 1.4 multiply_reduce_fusion.6
  365.8 1.5 fusion.96
  368.8 1.4 multiply_reduce_fusion.6
  370.2 1.5 fusion.96
  373.2 1.4 multiply_reduce_fusion.6
  374.6 1.5 fusion.96
  377.7 1.4 multiply_reduce_fusion.6
  379.1 1.5 fusion.96
  381.2 1.2 exponential_multiply_fusion
  382.4 1.9 convolution_bitcast_fusion.2
  384.3 1.9 convolution_bitcast_fusion.1
  386.9 7.9 %while.43 = (s32[]{:T(128)}, f32[2,1,64,128]{3,2,1,0:T(8,128)S(1)}, bf16[5,2,1,64,128]{4,3,1,2,0:T(8,128)(2,1)}, f32[5,2,1,64]{3,1,2,0:T(2,128)S(1)}, f32[5,2,1,...) while((s32[]{:T(128)}, f32[2,1,64,128]{3,2,1,0:T(8,128)S(1)}, ...), condition=%wide.region_10.11_spmd.clone, body=%wide.region_9.10_spmd.clone.sunk | while | flops 65540 | bytes 296576 | solution.py:130
  387.5 0.9 fusion.98
  389.1 0.9 fusion.98
  390.7 0.9 fusion.98
  392.2 0.9 fusion.98
  393.8 0.9 fusion.98
  395.5 7.9 %while.42 = (s32[]{:T(128)}, f32[2,1,64,128]{3,2,1,0:T(8,128)S(1)}, bf16[5,2,1,64,128]{4,3,1,2,0:T(8,128)(2,1)}, f32[5,2,1,64]{3,1,2,0:T(2,128)S(1)}, f32[5,2,1,64,128]{4,3,1,2,0:T(8,128)}, /*index=5*/s32[]{:T(128)}, s32[]{:T(128)}) while((s32[]{:T(128)}, f32[2,1,64,128]{3,2,1,0:T(8,128)S(1)}, ...), condition=%wide.region_8.9_spmd.clone, body=%wide.region_7.8_spmd.clone.sunk | while | flops 65539 | bytes 296556 | solution.py:129
  396.1 0.9 fusion.97
  403.4 1.2 fusion.46
  404.6 2.2 multiply_reduce_fusion.4
  406.8 2.0 fusion.42
  408.8 1.9 convolution_convert_fusion.2
  410.7 35.6 %all_to_all.40 = bf16[8,80,2048]{2,1,0:T(8,128)(2,1)S(1)} all-to-all(bf16[8,80,2048]{2,1,0:T(8,128)(2,1)S(1)} %bitcast.203), channel_id=1, replica_groups=mesh['grp'=2,'fs'=16,'tp'=8] {'tp'}, dimensions={0} | all-to-all | bytes 5242880 | tf_op jit(solution)/shard_map/all_to_all | solution.py:38
  447.6 35.5 %all_to_all.41 = bf16[8,80,2048]{2,1,0:T(8,128)(2,1)S(1)} all-to-all(bf16[8,80,2048]{2,1,0:T(8,128)(2,1)S(1)} %broadcast_in_dim.70), channel_id=1, replica_groups=mesh['grp'=2,'fs'=16,'tp'=8] {'tp'}, dimensions={0} | all-to-all | bytes 5242880 | tf_op jit(solution)/shard_map/all_to_all | solution.py:23
  483.1 1.5 copy-done.5
  484.7 3.4 fusion.13
  488.1 9.7 %convolution_convert_fusion = bf16[640,2048]{1,0:T(8,128)(2,1)} fusion(bf16[640,2048]{0,1:T(8,128)(2,1)S(1)} %bitcast.216, f32[640,640]{0,1:T(8,128)} %fusion.13, bf16[640,2048]{1,0:T(8,128)(2,1)} %bitcast.221, bf16[2048,1280]{1,0:T(8,128)(2,1)} %all-gather.3.cloned.1.call-done), kind=kOutput, calls=%fused_computation.26 | convolution fusion | flops 3359211520 | bytes 12124160 | tf_op jit(solution)/shard_map/dot_general | solution.py:65
  497.8 36.4 %all_to_all.42 = bf16[8,80,2048]{2,1,0:T(8,128)(2,1)S(1)} all-to-all(bf16[8,80,2048]{2,1,0:T(8,128)(2,1)} %bitcast.222), channel_id=1, replica_groups=mesh['grp'=2,'fs'=16,'tp'=8] {'tp'}, dimensions={0} | all-to-all | bytes 5242880 | tf_op jit(solution)/shard_map/all_to_all | solution.py:38
  (139 shorter events, 36.9 us)
Async XLA Ops:
  6.5 321.6 %copy-start = (bf16[2048,32]{0,1:T(8,128)(2,1)S(1)}, bf16[2048,32]{0,1:T(8,128)(2,1)}, u32[]{:S(2)}) copy-start(bf16[2048,32]{0,1:T(8,128)(2,1)} %param.28) | copy-start | bytes 393220
  9.4 24.1 %copy-start.7 = (bf16[128,640]{1,0:T(8,128)(2,1)S(1)}, bf16[128,640]{1,0:T(8,128)(2,1)}, u32[]{:S(2)}) copy-start(bf16[128,640]{1,0:T(8,128)(2,1)} %param.22) | copy-start | bytes 491524
  9.4 24.1 %copy-start.8 = (bf16[128,640]{1,0:T(8,128)(2,1)S(1)}, bf16[128,640]{1,0:T(8,128)(2,1)}, u32[]{:S(2)}) copy-start(bf16[128,640]{1,0:T(8,128)(2,1)} %param.21) | copy-start | bytes 491524
  9.4 24.9 %copy-start.9 = (bf16[640,128]{1,0:T(8,128)(2,1)S(1)}, bf16[640,128]{1,0:T(8,128)(2,1)}, u32[]{:S(2)}) copy-start(bf16[640,128]{1,0:T(8,128)(2,1)} %param.23) | copy-start | bytes 491524
  9.4 56.0 %all-to-all-start = ((bf16[8,80,2048]{2,1,0:T(8,128)(2,1)}), bf16[8,80,2048]{2,1,0:T(8,128)(2,1)S(1)}, u32[]{:S(2)}, u32[]{:S(2)}) async-start(bf16[8,80,2048]{2,1,0:T(8,128)(2,1)} %broadcast_in_dim.65), calls=%async_computation | async-start | bytes 5242880 | tf_op jit(solution)/shard_map/all_to_all | solution.py:23
  33.5 181.8 %all-gather.3.cloned.1.call-start = ((), (), s32[]{:S(2)}) async-start(), calls=%async_computation.8 | async-start | bytes 5570560 | tf_op jit(solution)/shard_map/all_gather | solution.py:44
  65.4 2.4 copy-start.4
  67.7 153.4 %all-to-all-start.1 = ((bf16[16,640,128]{1,2,0:T(8,128)(2,1)}), bf16[16,640,128]{1,2,0:T(8,128)(2,1)S(1)}, u32[]{:S(2)}, u32[]{:S(2)}) async-start(bf16[16,640,128]{1,2,0:T(8,128)(2,1)} %stack.2), calls=%async_computation.1 | async-start | bytes 5242880 | tf_op jit(solution)/shard_map/all_to_all | solution.py:159
  221.2 10.8 %copy-start.2 = (bf16[16,640,128]{1,2,0:T(8,128)(2,1)}, bf16[16,640,128]{1,2,0:T(8,128)(2,1)S(1)}, u32[]{:S(2)}) copy-start(bf16[16,640,128]{1,2,0:T(8,128)(2,1)S(1)} %all-to-all-done.1) | copy-start | bytes 7864324
  232.0 10.1 %copy-start.13 = (bf16[128,64]{0,1:T(8,128)(2,1)S(1)}, bf16[128,64]{0,1:T(8,128)(2,1)}, u32[]{:S(2)}) copy-start(bf16[128,64]{0,1:T(8,128)(2,1)} %param.25) | copy-start | bytes 49156
  232.0 10.3 %copy-start.14 = (bf16[128,64]{0,1:T(8,128)(2,1)S(1)}, bf16[128,64]{0,1:T(8,128)(2,1)}, u32[]{:S(2)}) copy-start(bf16[128,64]{0,1:T(8,128)(2,1)} %param.24) | copy-start | bytes 49156
  232.0 10.4 %copy-start.10 = (bf16[128,128]{1,0:T(8,128)(2,1)S(1)}, bf16[128,128]{1,0:T(8,128)(2,1)}, u32[]{:S(2)}) copy-start(bf16[128,128]{1,0:T(8,128)(2,1)} %param.27) | copy-start | bytes 98308
  232.0 10.4 %copy-start.11 = (bf16[128,128]{1,0:T(8,128)(2,1)S(1)}, bf16[128,128]{1,0:T(8,128)(2,1)}, u32[]{:S(2)}) copy-start(bf16[128,128]{1,0:T(8,128)(2,1)} %param.26) | copy-start | bytes 98308
  232.0 41.9 %all-to-all-start.2 = ((bf16[8,80,2048]{2,1,0:T(8,128)(2,1)}), bf16[8,80,2048]{2,1,0:T(8,128)(2,1)S(1)}, u32[]{:S(2)}, u32[]{:S(2)}) async-start(bf16[8,80,2048]{2,1,0:T(8,128)(2,1)} %bitcast.219), calls=%async_computation.2 | async-start | bytes 5242880 | tf_op jit(solution)/shard_map/all_to_all | solution.py:38
  242.1 32.3 %copy-start.1 = (bf16[80,2048]{1,0:T(8,128)(2,1)S(1)}, bf16[80,2048]{1,0:T(8,128)(2,1)}, u32[]{:S(2)}) copy-start(bf16[80,2048]{1,0:T(8,128)(2,1)} %param.20) | copy-start | bytes 983044
  242.1 80.2 %all-gather.5.cloned.1.call-start = ((), (), s32[]{:S(2)}) async-start(), calls=%async_computation.9 | async-start | bytes 1671168 | tf_op jit(solution)/shard_map/all_gather | solution.py:44
  276.9 4.7 copy-start.12
  276.9 36.6 %all-to-all-start.3 = ((bf16[8,80,2048]{2,1,0:T(8,128)(2,1)}), bf16[8,80,2048]{2,1,0:T(8,128)(2,1)S(1)}, u32[]{:S(2)}, u32[]{:S(2)}) async-start(bf16[8,80,2048]{2,1,0:T(8,128)(2,1)} %broadcast_in_dim.67), calls=%async_computation.3 | async-start | bytes 5242880 | tf_op jit(solution)/shard_map/all_to_all | solution.py:23
  314.4 94.4 %all-to-all-start.4 = ((bf16[16,128,128]{1,2,0:T(8,128)(2,1)}), bf16[16,128,128]{1,2,0:T(8,128)(2,1)}, u32[]{:S(2)}, u32[]{:S(2)}) async-start(bf16[16,128,128]{1,2,0:T(8,128)(2,1)} %broadcast_in_dim.69), calls=%async_computation.4 | async-start | bytes 1048576 | tf_op jit(solution)/shard_map/all_to_all | solution.py:23
  324.2 3.9 copy-start.6
  324.3 3.9 copy-start.15
  324.3 3.9 copy-start.16
  394.8 12.0 %copy-start.17 = (f32[128]{0:T(128)S(1)}, f32[128]{0:T(128)}, u32[]{:S(2)}) copy-start(f32[128]{0:T(128)} %param.32) | copy-start | bytes 1540
  446.7 38.0 %slice-start = ((s8[5242880]{0:T(1024)(128)(4,1)}), s8[4194304]{0:T(1024)(128)(4,1)S(1)}, s32[]{:S(2)}) async-start(s8[5242880]{0:T(1024)(128)(4,1)} %bitcast.230), calls=%async_computation.10 | async-start | bytes 8388608
  447.3 37.4 %slice-start.1 = ((s8[5242880]{0:T(1024)(128)(4,1)}), s8[1048576]{0:T(1024)(128)(4,1)S(1)}, s32[]{:S(2)}) async-start(s8[5242880]{0:T(1024)(128)(4,1)} %bitcast.230), calls=%async_computation.11 | async-start | bytes 2097152
  483.1 1.5 copy-start.5
  484.7 3.4 copy-start.3
Sparse Core Ops, SparseCore 0:
  36.1 179.1 all-gather.2
  244.7 57.4 all-gather.4
